TPU v7x, 32 devices: a whole 2x2x4 slice. The times are simulated.
32 devices in a mesh: ep: 8 (over z, x), tp: 4 (over y, core).
Axes of the slice: x: 2, y: 2, z: 4, core: 2. Of those that a mesh axis runs over, the one named last changes fastest.
Arguments:
- mix_bgate: bfloat16 [2048, 1024], P('ep', 'tp'), may hold values from -6 to 6
- mix_cgate: bfloat16 [2048, 1024], P('ep', 'tp'), may hold values from -6 to 6
- mix_input: bfloat16 [2048, 1024], P('ep', 'tp'), may hold values from -6 to 6
- conv_taps: float32 [3, 1024], P(None, 'tp'), may hold values from -3.5 to 3.5
- mix_out_w: bfloat16 [1024, 2048], P('tp'), may hold values from -0.1875 to 0.1875
- moe_x: bfloat16 [2048, 2048], P('ep', 'tp'), may hold values from -6 to 6
- moe_gain: float32 [2048], replicated, may hold values from 0.1 to 1.9
- routes: int32 [2048, 2], P('ep'), may hold values from 0 to 7, all different within a row; in each aligned block of 256 rows (0 to 255, 256 to 511, ...) at most 96 rows name the same one
- route_w: float32 [2048, 2], P('ep'), may hold values from 0.2 to 1
- w_gate: bfloat16 [8, 2048, 3584], P('ep', None, 'tp'), may hold values from -0.125 to 0.125
- w_up: bfloat16 [8, 2048, 3584], P('ep', None, 'tp'), may hold values from -0.125 to 0.125
- w_down: bfloat16 [8, 3584, 2048], P('ep', 'tp'), may hold values from -0.09375 to 0.09375
Outputs:
- mixed: bfloat16 [2048, 2048], P(('ep', 'tp'))
- routed: bfloat16 [2048, 2048], P('ep', 'tp')
Inputs may be any that keep to these rules, and one draw needn't show every extreme that they name: `routes`: among the 256 rows of one index of ep, each row names 2 different experts and no expert is named by more than 96 rows; in every draw some expert is named by exactly 96 rows of some index.
All inputs are finite; a program needn't handle non-finite values.
Results may differ from a plain program's by a relative error of at most 0.012.
Values may be sent and summed in bfloat16 or wider, within the bound.
A program may use at most 64 MiB of HBM per device.

v0:
```python
import jax
import jax.numpy as jnp
from jax import lax
from jax.sharding import PartitionSpec as P


def shifted(block, axis, distance):
    devices = range(lax.axis_size(axis))
    route = [(i - distance, i) for i in devices if i - distance in devices]
    return lax.ppermute(block, axis, route)


def rms_rows(values, gain):
    wide = values.astype(jnp.float32)
    scale = lax.rsqrt(jnp.mean(wide * wide, axis=-1, keepdims=True) + 1e-06)
    return (wide * scale * gain).astype(jnp.bfloat16)


def conv_mixer(mix_bgate, mix_cgate, mix_input, conv_taps, mix_out_w):
    length = mix_input.shape[0]
    reach = conv_taps.shape[0] - 1
    tail = jnp.stack([mix_cgate[length - reach :], mix_input[length - reach :]])
    before = shifted(tail, "ep", 1)
    gates_c = jnp.concatenate([before[0], mix_cgate], 0).astype(jnp.float32)
    inputs_h = jnp.concatenate([before[1], mix_input], 0).astype(jnp.float32)
    prod = gates_c * inputs_h
    conv = conv_taps[0] * prod[0:length]
    for j in range(1, reach + 1):
        conv = conv + conv_taps[j] * prod[j : j + length]
    gated = (mix_bgate.astype(jnp.float32) * conv).astype(jnp.bfloat16)
    return lax.psum_scatter(
        jnp.dot(gated, mix_out_w, preferred_element_type=jnp.float32).astype(jnp.bfloat16),
        "tp",
        scatter_dimension=0,
        tiled=True,
    )


def expert_layer(moe_x, moe_gain, routes, route_w, w_gate, w_up, w_down):
    whole = lax.all_gather(moe_x, "tp", axis=1, tiled=True)
    normed = rms_rows(whole, moe_gain)
    ntok, width = normed.shape
    top = routes.shape[1]
    n_ep = lax.axis_size("ep")
    n_tp = lax.axis_size("tp")
    per_dev = w_gate.shape[0]
    experts = per_dev * n_ep
    cap = 4 * ((3 * ntok * top + 8 * experts - 1) // (8 * experts))
    flat = routes.reshape(-1)
    onehot = (flat[:, None] == jnp.arange(experts, dtype=jnp.int32)[None, :]).astype(jnp.int32)
    earlier = jnp.cumsum(onehot, axis=0) - onehot
    slot = jnp.sum(earlier * onehot, axis=1)
    place = flat * cap + slot
    source = (
        jnp.full((experts * cap,), ntok, jnp.int32)
        .at[place]
        .set(jnp.arange(ntok * top, dtype=jnp.int32) // top)
    )
    padded = jnp.concatenate([normed, jnp.zeros((1, width), jnp.bfloat16)], 0)
    outgoing = padded[source].reshape(n_ep, per_dev, cap, width)
    part = cap // n_tp
    mine = lax.dynamic_slice_in_dim(outgoing, lax.axis_index("tp") * part, part, 2)
    landed = lax.all_to_all(mine, "ep", split_axis=0, concat_axis=0, tiled=True)
    arrived = lax.all_gather(landed, "tp", axis=2, tiled=True)
    gate = jnp.einsum("secd,edf->secf", arrived, w_gate, preferred_element_type=jnp.float32)
    upper = jnp.einsum("secd,edf->secf", arrived, w_up, preferred_element_type=jnp.float32)
    hidden = (jax.nn.silu(gate) * upper).astype(jnp.bfloat16)
    down = jnp.einsum("secf,efd->secd", hidden, w_down, preferred_element_type=jnp.float32)
    summed = lax.psum_scatter(down.astype(jnp.bfloat16), "tp", scatter_dimension=3, tiled=True)
    returned = lax.all_to_all(summed, "ep", split_axis=0, concat_axis=0, tiled=True)
    flat_back = returned.reshape(experts * cap, width // n_tp)
    picked = flat_back[place].astype(jnp.float32).reshape(ntok, top, width // n_tp)
    return jnp.sum(picked * route_w[:, :, None], axis=1).astype(jnp.bfloat16)


def body(
    mix_bgate,
    mix_cgate,
    mix_input,
    conv_taps,
    mix_out_w,
    moe_x,
    moe_gain,
    routes,
    route_w,
    w_gate,
    w_up,
    w_down,
):
    mixed = conv_mixer(mix_bgate, mix_cgate, mix_input, conv_taps, mix_out_w)
    routed = expert_layer(moe_x, moe_gain, routes, route_w, w_gate, w_up, w_down)
    return (mixed, routed)


def solution(mesh):
    in_specs = (
        P("ep", "tp"),
        P("ep", "tp"),
        P("ep", "tp"),
        P(None, "tp"),
        P("tp", None),
        P("ep", "tp"),
        P(),
        P("ep", None),
        P("ep", None),
        P("ep", None, "tp"),
        P("ep", None, "tp"),
        P("ep", "tp", None),
    )
    out_specs = (P(("ep", "tp"), None), P("ep", "tp"))
    return jax.shard_map(body, mesh=mesh, in_specs=in_specs, out_specs=out_specs, check_vma=False)
```

profile of v0, /device:TPU:0, one launch (start us, length us, event | category | flops | bytes accessed | tf_op | source)
XLA Modules:
  0.0 185.2 jit_solution(3375936974495529147)
XLA Ops:
  7.2 0.0 copy-start
  7.2 0.0 all-gather.3.cloned.1.call-start
  7.2 0.7 all-gather.3.cloned.1.call-update
  7.9 0.0 all-gather.5.cloned.1.call-start
  8.0 0.8 copy.20
  8.8 0.1 eq.29
  8.9 0.1 eq.25
  9.1 1.1 reduce-window.6
  10.2 0.2 slice_reduce_fusion
  10.5 0.7 broadcast_multiply_fusion
  11.2 0.1 copy.19
  11.3 0.1 mul.110
  11.5 0.1 fusion.43
  11.6 2.4 %scatter_custom_fusion = s32[768]{0:T(1024)S(1)} fusion(s32[512]{0:T(512)S(1)} %bitcast.108, s32[512]{0:T(512)S(1)} %add_select_fusion, s32[]{:T(128)} %constant.40.clone.1), kind=kCustom, calls=%fused_computation.57 | custom fusion | bytes 3076 | tf_op jit(solution)/shard_map/scatter | solution.py:57
  14.1 15.0 %all-gather.3.cloned.1.call-done = bf16[256,2048]{1,0:T(8,128)(2,1)} async-done(((bf16[256,512]{1,0:T(8,128)(2,1)}), bf16[256,2048]{1,0:T(8,128)(2,1)}) %all-gather.3.cloned.1.call-update) | async-done | bytes 1048592 | tf_op jit(solution)/shard_map/all_gather | solution.py:40
  29.0 1.5 fusion.18
  30.6 1.5 fusion.20
  32.1 0.1 concatenate.11
  32.2 4.3 %gather_fusion = bf16[768,2048]{1,0:T(8,128)(2,1)} fusion(bf16[257,2048]{1,0:T(8,128)(2,1)S(1)} %concatenate.11, s32[1024]{0:T(1024)S(1)} %pad_clamp_fusion.1), kind=kCustom, calls=%fused_computation | custom fusion | bytes 6294528 | tf_op jit(solution)/shard_map/gather | solution.py:60
  36.5 1.2 constant_dynamic-slice_fusion
  37.7 25.9 %all_to_all.10 = bf16[8,1,24,2048]{3,2,1,0:T(8,128)(2,1)} all-to-all(bf16[8,1,24,2048]{3,2,1,0:T(8,128)(2,1)S(1)} %constant_dynamic-slice_fusion), channel_id=1, replica_groups=mesh['ep'=8,'tp'=4] {'ep'}, dimensions={0} | all-to-all | bytes 1572864 | tf_op jit(solution)/shard_map/all_to_all | solution.py:63
  63.6 0.0 all-gather.5.cloned.1.call-update
  63.6 0.0 reduce-scatter.5.cloned.1.call-start
  63.7 26.7 %all-gather.5.cloned.1.call-done = bf16[8,1,96,2048]{3,2,0,1:T(8,128)(2,1)} async-done(((bf16[8,1,24,2048]{3,2,0,1:T(8,128)(2,1)}), bf16[8,1,96,2048]{3,2,0,1:T(8,128)(2,1)}) %all-gather.5.cloned.1.call-update) | async-done | bytes 3145744 | tf_op jit(solution)/shard_map/all_gather | solution.py:64
  90.4 8.0 %fusion.4 = f32[8,96,896]{2,1,0:T(8,128)} fusion(bf16[1,2048,896]{2,1,0:T(8,128)(2,1)} %param.21, bf16[8,1,96,2048]{3,2,0,1:T(8,128)(2,1)} %all-gather.5.cloned.1.call-done), kind=kOutput, calls=%fused_computation.7 | convolution fusion | flops 2818572288 | bytes 9568256 | tf_op jit(solution)/shard_map/secd,edf->secf/dot_general | solution.py:65
  98.4 12.1 %fusion.11 = bf16[8,1,96,2048]{3,2,0,1:T(8,128)(2,1)} fusion(bf16[1,896,2048]{2,1,0:T(8,128)(2,1)} %param.23, bf16[1,2048,896]{2,1,0:T(8,128)(2,1)} %param.22, bf16[8,1,96,2048]{3,2,0,1:T(8,128)(2,1)} %all-gather.5.cloned.1.call-done, f32[8,96,896]{2,1,0:T(8,128)} %fusion.4), kind=kOutput, calls=%fused_computation.12 | convolution fusion | flops 5642846208 | bytes 16384000 | tf_op jit(solution)/shard_map/secf,efd->secd/dot_general | solution.py:68
  110.5 0.0 copy-start.3
  110.5 0.0 reduce-scatter.5.cloned.1.call-update
  110.5 0.0 copy-start.5
  110.5 0.0 reduce-scatter.3.cloned.1.call-start
  110.6 0.8 copy-done.1
  111.4 0.1 copy-done.2
  111.5 3.4 %collective-permute-start = (bf16[2,2,256]{2,1,0:T(2,128)(2,1)S(1)}, bf16[2,2,256]{2,1,0:T(2,128)(2,1)S(1)}, u32[]{:S(2)}, u32[]{:S(2)}) collective-permute-start(bf16[2,2,256]{2,1,0:T(2,128)(2,1)S(1)} %pad_maximum_fusion), channel_id=1, source_target_pairs={{0,4},{4,8},{8,12},{12,16},{16,20},{20,24},{24,28},{1,5},{5,9},{9,... | collective-permute-start | bytes 6152 | tf_op jit(solution)/shard_map/ppermute | solution.py:10
  114.9 0.0 copy-done.4
  114.9 1.3 collective-permute-done
  116.2 0.1 convert_multiply_fusion.2
  116.2 0.0 copy-done
  116.2 0.0 copy-done.3
  116.2 1.5 convolution_convert_fusion
  117.7 0.0 reduce-scatter.3.cloned.1.call-update
  117.7 30.7 %reduce-scatter.5.cloned.1.call-done = bf16[8,1,96,512]{3,2,0,1:T(8,128)(2,1)} async-done(((bf16[8,1,96,2048]{3,2,0,1:T(8,128)(2,1)}), bf16[8,1,96,512]{3,2,0,1:T(8,128)(2,1)}) %reduce-scatter.5.cloned.1.call-update) | async-done | bytes 786448 | tf_op jit(solution)/shard_map/reduce_scatter | solution.py:69
  148.4 5.5 %all-to-all-start.1 = ((bf16[8,1,96,512]{3,2,1,0:T(8,128)(2,1)}), bf16[8,1,96,512]{3,2,1,0:T(8,128)(2,1)S(1)}, u32[]{:S(2)}, u32[]{:S(2)}) async-start(bf16[8,1,96,512]{3,2,1,0:T(8,128)(2,1)} %bitcast.107), calls=%async_computation.3 | async-start | bytes 1572864 | tf_op jit(solution)/shard_map/all_to_all | solution.py:70
  153.9 0.0 copy-done.5
  153.9 0.1 copy.25
  154.1 19.9 %all-to-all-done.1 = bf16[8,1,96,512]{3,2,1,0:T(8,128)(2,1)S(1)} async-done(((bf16[8,1,96,512]{3,2,1,0:T(8,128)(2,1)}), bf16[8,1,96,512]{3,2,1,0:T(8,128)(2,1)S(1)}, u32[]{:S(2)}, u32[]{:S(2)}) %all-to-all-start.1) | async-done | bytes 786464 | tf_op jit(solution)/shard_map/all_to_all | solution.py:70
  174.0 2.0 %gather_fusion.1 = bf16[512,512]{1,0:T(8,128)(2,1)S(1)} fusion(bf16[768,512]{1,0:T(8,128)(2,1)S(1)} %bitcast.104, s32[1024]{0:T(1024)S(1)} %pad_clamp_fusion), kind=kCustom, calls=%fused_computation.1 | custom fusion | bytes 1050624 | tf_op jit(solution)/shard_map/gather | solution.py:72
  176.0 0.7 reshape.98
  176.6 2.1 %multiply_reduce_fusion = bf16[256,512]{1,0:T(8,128)(2,1)} fusion(f32[256,2,512]{2,1,0:T(2,128)S(1)} %reshape.98, f32[256,2]{1,0:T(8,128)S(1)} %copy.25), kind=kLoop, calls=%fused_computation.27 | loop fusion | flops 393216 | bytes 1312768 | tf_op jit(solution)/shard_map/reduce_sum | solution.py:73
  (17 shorter events, 0.1 us)
Async XLA Ops:
  7.2 109.1 %copy-start = (bf16[256,2048]{1,0:T(8,128)(2,1)S(1)}, bf16[256,2048]{1,0:T(8,128)(2,1)}, u32[]{:S(2)}) copy-start(bf16[256,2048]{1,0:T(8,128)(2,1)} %param.16) | copy-start | bytes 3145732
  7.2 21.9 %all-gather.3.cloned.1.call-start = ((), (), s32[]{:S(2)}) async-start(), calls=%async_computation.5 | async-start | bytes 1310720 | tf_op jit(solution)/shard_map/all_gather | solution.py:40
  7.9 82.5 %all-gather.5.cloned.1.call-start = ((), (), s32[]{:S(2)}) async-start(), calls=%async_computation.6 | async-start | bytes 3932160 | tf_op jit(solution)/shard_map/all_gather | solution.py:64
  63.6 84.8 %reduce-scatter.5.cloned.1.call-start = ((), (), s32[]{:S(2)}) async-start(), calls=%async_computation.7 | async-start | bytes 3932160 | tf_op jit(solution)/shard_map/reduce_scatter | solution.py:69
  110.5 0.9 copy-start.1
  110.5 1.0 copy-start.2
  110.5 4.4 %copy-start.4 = (f32[3,256]{1,0:T(4,128)S(1)}, f32[3,256]{1,0:T(4,128)}, u32[]{:S(2)}) copy-start(f32[3,256]{1,0:T(4,128)} %param.15) | copy-start | bytes 9220
  110.5 5.7 %copy-start.3 = (bf16[256,256]{1,0:T(8,128)(2,1)S(1)}, bf16[256,256]{1,0:T(8,128)(2,1)}, u32[]{:S(2)}) copy-start(bf16[256,256]{1,0:T(8,128)(2,1)} %param.12) | copy-start | bytes 393220
  110.5 43.4 %copy-start.5 = (f32[256,2]{0,1:T(2,128)S(1)}, f32[256,2]{0,1:T(2,128)}, u32[]{:S(2)}) copy-start(f32[256,2]{0,1:T(2,128)} %param.20) | copy-start | bytes 6148
  110.5 68.1 %reduce-scatter.3.cloned.1.call-start = ((), (), s32[]{:S(2)}) async-start(), calls=%async_computation.4 | async-start | bytes 1310720 | tf_op jit(solution)/shard_map/reduce_scatter | solution.py:31
  111.5 4.7 %collective-permute-start = (bf16[2,2,256]{2,1,0:T(2,128)(2,1)S(1)}, bf16[2,2,256]{2,1,0:T(2,128)(2,1)S(1)}, u32[]{:S(2)}, u32[]{:S(2)}) collective-permute-start(bf16[2,2,256]{2,1,0:T(2,128)(2,1)S(1)} %pad_maximum_fusion), channel_id=1, source_target_pairs={{0,4},{4,8},{8,12},{12,16},{16,20},{20,24},{24,28},{1,5},{5,9},{9,... | collective-permute-start | bytes 6152 | tf_op jit(solution)/shard_map/ppermute | solution.py:10
  148.4 25.6 %all-to-all-start.1 = ((bf16[8,1,96,512]{3,2,1,0:T(8,128)(2,1)}), bf16[8,1,96,512]{3,2,1,0:T(8,128)(2,1)S(1)}, u32[]{:S(2)}, u32[]{:S(2)}) async-start(bf16[8,1,96,512]{3,2,1,0:T(8,128)(2,1)} %bitcast.107), calls=%async_computation.3 | async-start | bytes 1572864 | tf_op jit(solution)/shard_map/all_to_all | solution.py:70
Sparse Core Ops, SparseCore 0:
  9.5 19.4 all-gather.2
  63.7 26.6 all-gather.4
  110.7 37.7 reduce-scatter.4
  151.4 24.7 reduce-scatter.2
where the time goes:
time: 186 us; the launch traced here: 185 us
  waiting for transfers between devices  94.3 us (51%)
  blocking collectives  25.9 us (14%)
  matrix products  21.5 us (12%)
  between operations  14 us (8%)
  local copies, waits for them, and re-layouts  13.3 us (7%)
  starting transfers between devices  9.05 us (5%)
  other arithmetic  7.18 us (4%)
    reduce_scatter x1, waiting for transfers between devices, expert_layer(): lax.psum_scatter(down.astype(jnp.bfloat16), 'tp', scatter_dimension=3, ti...  30.7 us
    all_gather x1, waiting for transfers between devices, expert_layer(): arrived = lax.all_gather(landed, 'tp', axis=2, tiled=True)  26.7 us
    all_to_all x1, blocking collectives, expert_layer(): landed = lax.all_to_all(mine, 'ep', split_axis=0, concat_axis=0, tiled=True)  25.9 us
    all_to_all x1, waiting for transfers between devices, expert_layer(): lax.all_to_all(summed, 'ep', split_axis=0, concat_axis=0, tiled=True)  19.9 us
    all_gather x1, waiting for transfers between devices, expert_layer(): whole = lax.all_gather(moe_x, 'tp', axis=1, tiled=True)  15 us
    dot_general x1, matrix products, expert_layer(): jnp.einsum('secf,efd->secd', hidden, w_down, preferred_element_type=jnp.f...  12.1 us
    dot_general x1, matrix products, expert_layer(): jnp.einsum('secd,edf->secf', arrived, w_gate, preferred_element_type=jnp....  8 us
    all_to_all x1, starting transfers between devices, expert_layer(): lax.all_to_all(summed, 'ep', split_axis=0, concat_axis=0, tiled=True)  5.52 us
  transfers between devices with their start and end apart: 6, of which 5 were waited for; matrix products, arithmetic and copies ran while one was open for 7% of the time, Pallas kernels for 0%

commit v1 on v0

--- a/solution.py
+++ b/solution.py
@@ -61,7 +61,12 @@
     part = cap // n_tp
     mine = lax.dynamic_slice_in_dim(outgoing, lax.axis_index("tp") * part, part, 2)
     landed = lax.all_to_all(mine, "ep", split_axis=0, concat_axis=0, tiled=True)
-    arrived = lax.all_gather(landed, "tp", axis=2, tiled=True)
+    ring = [landed]
+    for hop in range(3):
+        ring.append(lax.ppermute(ring[-1], "tp", [(dev, (dev + 1) % 4) for dev in range(4)]))
+    arrived = jnp.roll(
+        jnp.concatenate(ring[::-1], axis=2), (lax.axis_index("tp") + 1) * ring[0].shape[2], axis=2
+    )
     gate = jnp.einsum("secd,edf->secf", arrived, w_gate, preferred_element_type=jnp.float32)
     upper = jnp.einsum("secd,edf->secf", arrived, w_up, preferred_element_type=jnp.float32)
     hidden = (jax.nn.silu(gate) * upper).astype(jnp.bfloat16)

time: 186 us -> 194 us (1.043)
  waiting for transfers between devices: 94.3 us -> 101 us
  local copies, waits for them, and re-layouts: 13.3 us -> 18 us
  matrix products: 21.5 us -> 18.6 us
    ppermute x0 -> x3, waiting for transfers between devices: none -> 34.3 us  [expert_layer(): lax.ppermute(ring[-1], 'tp', [(dev, (dev + 1) % 4) for dev in range(4)])]
    all_gather x1 -> x0, waiting for transfers between devices: 26.7 us -> none  [expert_layer(): arrived = lax.all_gather(landed, 'tp', axis=2, tiled=True)]
    unnamed x14 -> x25, local copies, waits for them, and re-layouts: 1.83 us -> 6.49 us
    dot_general x1, matrix products: 8 us -> 4.92 us  [expert_layer(): jnp.einsum('secd,edf->secf', arrived, w_gate, preferred_element_type=jnp....]
  transfers between devices with their start and end apart: 6 -> 8, of which waited for: 5 -> 7; matrix products, arithmetic and copies ran while one was open for 7% -> 6% of each run, Pallas kernels for 0% -> 0%
where the time goes in v1:
time: 194 us; the launch traced here: 193 us
  waiting for transfers between devices  101 us (52%)
  blocking collectives  25.8 us (13%)
  matrix products  18.6 us (10%)
  local copies, waits for them, and re-layouts  18 us (9%)
  between operations  14 us (7%)
  starting transfers between devices  9 us (5%)
  other arithmetic  7.18 us (4%)
    ppermute x3, waiting for transfers between devices, expert_layer(): lax.ppermute(ring[-1], 'tp', [(dev, (dev + 1) % 4) for dev in range(4)])  34.3 us
    reduce_scatter x1, waiting for transfers between devices, expert_layer(): lax.psum_scatter(down.astype(jnp.bfloat16), 'tp', scatter_dimension=3, ti...  29.6 us
    all_to_all x1, blocking collectives, expert_layer(): landed = lax.all_to_all(mine, 'ep', split_axis=0, concat_axis=0, tiled=True)  25.8 us
    all_to_all x1, waiting for transfers between devices, expert_layer(): lax.all_to_all(summed, 'ep', split_axis=0, concat_axis=0, tiled=True)  19.9 us
    all_gather x1, waiting for transfers between devices, expert_layer(): whole = lax.all_gather(moe_x, 'tp', axis=1, tiled=True)  15 us
    dot_general x1, matrix products, expert_layer(): jnp.einsum('secf,efd->secd', hidden, w_down, preferred_element_type=jnp.f...  12.2 us
    unnamed x25, local copies, waits for them, and re-layouts  6.49 us
    all_to_all x1, starting transfers between devices, expert_layer(): lax.all_to_all(summed, 'ep', split_axis=0, concat_axis=0, tiled=True)  5.51 us
  transfers between devices with their start and end apart: 8, of which 7 were waited for; matrix products, arithmetic and copies ran while one was open for 6% of the time, Pallas kernels for 0%

profile of v1, /device:TPU:0, one launch (start us, length us, event | category | flops | bytes accessed | tf_op | source)
XLA Modules:
  0.0 193.4 jit_solution(10172168839262738168)
XLA Ops:
  7.2 0.0 all-gather.2.cloned.1.call-start
  7.2 0.7 all-gather.2.cloned.1.call-update
  7.9 0.0 reduce-scatter.5.cloned.1.call-start
  8.0 0.8 copy.20
  8.8 0.1 eq.32
  8.9 0.1 eq.28
  9.1 1.1 reduce-window.6
  10.2 0.2 slice_reduce_fusion
  10.5 0.7 broadcast_multiply_fusion
  11.2 0.1 copy.19
  11.3 0.1 mul.113
  11.5 0.1 fusion.45
  11.6 2.4 %scatter_custom_fusion = s32[768]{0:T(1024)S(1)} fusion(s32[512]{0:T(512)S(1)} %bitcast.106, s32[512]{0:T(512)S(1)} %add_select_fusion, s32[]{:T(128)} %constant.57.clone.1), kind=kCustom, calls=%fused_computation.67 | custom fusion | bytes 3076 | tf_op jit(solution)/shard_map/scatter | solution.py:57
  14.1 15.0 %all-gather.2.cloned.1.call-done = bf16[256,2048]{1,0:T(8,128)(2,1)} async-done(((bf16[256,512]{1,0:T(8,128)(2,1)}), bf16[256,2048]{1,0:T(8,128)(2,1)}) %all-gather.2.cloned.1.call-update) | async-done | bytes 1048592 | tf_op jit(solution)/shard_map/all_gather | solution.py:40
  29.1 1.5 fusion.20
  30.6 1.5 fusion.22
  32.1 0.1 concatenate.17
  32.2 4.3 %gather_fusion = bf16[768,2048]{1,0:T(8,128)(2,1)} fusion(bf16[257,2048]{1,0:T(8,128)(2,1)S(1)} %concatenate.17, s32[1024]{0:T(1024)S(1)} %pad_clamp_fusion.1), kind=kCustom, calls=%fused_computation | custom fusion | bytes 6294528 | tf_op jit(solution)/shard_map/gather | solution.py:60
  36.5 1.2 constant_dynamic-slice_fusion
  37.7 25.8 %all_to_all.10 = bf16[8,1,24,2048]{3,2,1,0:T(8,128)(2,1)S(1)} all-to-all(bf16[8,1,24,2048]{3,2,1,0:T(8,128)(2,1)S(1)} %constant_dynamic-slice_fusion), channel_id=1, replica_groups=mesh['ep'=8,'tp'=4] {'ep'}, dimensions={0} | all-to-all | bytes 1572864 | tf_op jit(solution)/shard_map/all_to_all | solution.py:63
  63.5 11.4 %collective-permute-done.1 = bf16[8,1,24,2048]{3,2,1,0:T(8,128)(2,1)S(1)} collective-permute-done((bf16[8,1,24,2048]{3,2,1,0:T(8,128)(2,1)S(1)}, bf16[8,1,24,2048]{3,2,1,0:T(8,128)(2,1)S(1)}, u32[]{:S(2)}, u32[]{:S(2)}) %collective-permute-start.1) | collective-permute-done | bytes 786464 | tf_op jit(solution)/shard_map/ppermute | solution.py:66
  74.9 11.4 %collective-permute-done.2 = bf16[8,1,24,2048]{3,2,1,0:T(8,128)(2,1)S(1)} collective-permute-done((bf16[8,1,24,2048]{3,2,1,0:T(8,128)(2,1)S(1)}, bf16[8,1,24,2048]{3,2,1,0:T(8,128)(2,1)S(1)}, u32[]{:S(2)}, u32[]{:S(2)}) %collective-permute-start.2) | collective-permute-done | bytes 786464 | tf_op jit(solution)/shard_map/ppermute | solution.py:66
  86.3 11.5 %collective-permute-done.3 = bf16[8,1,24,2048]{3,2,1,0:T(8,128)(2,1)} collective-permute-done((bf16[8,1,24,2048]{3,2,1,0:T(8,128)(2,1)S(1)}, bf16[8,1,24,2048]{3,2,1,0:T(8,128)(2,1)}, u32[]{:S(2)}, u32[]{:S(2)}) %collective-permute-start.3) | collective-permute-done | bytes 786464 | tf_op jit(solution)/shard_map/ppermute | solution.py:66
  97.8 1.2 constant_dynamic-update-slice_fusion.7
  99.0 0.1 constant_dynamic-update-slice_fusion.6
  99.1 0.1 constant_dynamic-update-slice_fusion.5
  99.2 0.1 constant_dynamic-update-slice_fusion.4
  99.3 1.3 constant_dynamic-update-slice_fusion.3
  100.6 0.1 constant_dynamic-update-slice_fusion.2
  100.7 0.1 constant_dynamic-update-slice_fusion.1
  100.8 0.1 constant_dynamic-update-slice_fusion
  100.8 2.6 %copy-done.4 = bf16[8,1,192,2048]{3,2,1,0:T(8,128)(2,1)} copy-done((bf16[8,1,192,2048]{3,2,1,0:T(8,128)(2,1)}, bf16[8,1,192,2048]{3,2,1,0:T(8,128)(2,1)S(1)}, u32[]{:S(2)}) %copy-start.4) | copy-done | bytes 6291480
  103.5 4.9 %fusion.4 = f32[8,96,896]{2,1,0:T(8,128)} fusion(bf16[1,2048,896]{2,1,0:T(8,128)(2,1)S(1)} %copy-done.7, bf16[8,1,192,2048]{3,2,1,0:T(8,128)(2,1)S(1)} %constant_dynamic-update-slice_fusion, s32[]{:T(128)S(6)} %select_n.40), kind=kOutput, calls=%fused_computation.7 | convolution fusion | flops 2818572288 | bytes 9568260 | tf_op jit(solution)/shard_map/secd,edf->secf/dot_general | solution.py:70
  108.4 12.2 %fusion.11 = bf16[8,1,96,2048]{3,2,0,1:T(8,128)(2,1)} fusion(bf16[1,896,2048]{2,1,0:T(8,128)(2,1)} %param.23, bf16[1,2048,896]{2,1,0:T(8,128)(2,1)} %param.22, bf16[8,1,192,2048]{3,2,1,0:T(8,128)(2,1)} %copy-done.4, s32[]{:T(128)S(6)} %select_n.40, f32[8,96,896]{2,1,0:T(8,128)} %fusion.4), kind=kOutput, calls=%fused_computation.12 | convolution fusion | flops 5642846208 | bytes 16384004 | tf_op jit(solution)/shard_map/secf,efd->secd/dot_general | solution.py:73
  120.6 0.0 reduce-scatter.5.cloned.1.call-update
  120.7 0.0 reduce-scatter.3.cloned.1.call-start
  120.8 3.4 %collective-permute-start = (bf16[2,2,256]{2,1,0:T(2,128)(2,1)S(1)}, bf16[2,2,256]{2,1,0:T(2,128)(2,1)S(1)}, u32[]{:S(2)}, u32[]{:S(2)}) collective-permute-start(bf16[2,2,256]{2,1,0:T(2,128)(2,1)S(1)} %pad_maximum_fusion), channel_id=1, source_target_pairs={{0,4},{4,8},{8,12},{12,16},{16,20},{20,24},{24,28},{1,5},{5,9},{9,... | collective-permute-start | bytes 6152 | tf_op jit(solution)/shard_map/ppermute | solution.py:10
  124.2 1.3 collective-permute-done
  125.4 0.1 convert_multiply_fusion.2
  125.5 1.5 convolution_convert_fusion
  127.0 0.0 reduce-scatter.3.cloned.1.call-update
  127.0 29.6 %reduce-scatter.5.cloned.1.call-done = bf16[8,1,96,512]{3,2,0,1:T(8,128)(2,1)} async-done(((bf16[8,1,96,2048]{3,2,0,1:T(8,128)(2,1)}), bf16[8,1,96,512]{3,2,0,1:T(8,128)(2,1)}) %reduce-scatter.5.cloned.1.call-update) | async-done | bytes 786448 | tf_op jit(solution)/shard_map/reduce_scatter | solution.py:74
  156.7 5.5 %all-to-all-start.1 = ((bf16[8,1,96,512]{3,2,1,0:T(8,128)(2,1)}), bf16[8,1,96,512]{3,2,1,0:T(8,128)(2,1)S(1)}, u32[]{:S(2)}, u32[]{:S(2)}) async-start(bf16[8,1,96,512]{3,2,1,0:T(8,128)(2,1)} %bitcast.105), calls=%async_computation.3 | async-start | bytes 1572864 | tf_op jit(solution)/shard_map/all_to_all | solution.py:75
  162.2 0.1 copy.24
  162.3 19.9 %all-to-all-done.1 = bf16[8,1,96,512]{3,2,1,0:T(8,128)(2,1)S(1)} async-done(((bf16[8,1,96,512]{3,2,1,0:T(8,128)(2,1)}), bf16[8,1,96,512]{3,2,1,0:T(8,128)(2,1)S(1)}, u32[]{:S(2)}, u32[]{:S(2)}) %all-to-all-start.1) | async-done | bytes 786464 | tf_op jit(solution)/shard_map/all_to_all | solution.py:75
  182.2 2.0 %gather_fusion.1 = bf16[512,512]{1,0:T(8,128)(2,1)S(1)} fusion(bf16[768,512]{1,0:T(8,128)(2,1)S(1)} %bitcast.103, s32[1024]{0:T(1024)S(1)} %pad_clamp_fusion), kind=kCustom, calls=%fused_computation.1 | custom fusion | bytes 1050624 | tf_op jit(solution)/shard_map/gather | solution.py:77
  184.2 0.7 reshape.98
  184.9 2.1 %multiply_reduce_fusion = bf16[256,512]{1,0:T(8,128)(2,1)} fusion(f32[256,2,512]{2,1,0:T(2,128)S(1)} %reshape.98, f32[256,2]{1,0:T(8,128)S(1)} %copy.24), kind=kLoop, calls=%fused_computation.29 | loop fusion | flops 393216 | bytes 1312768 | tf_op jit(solution)/shard_map/reduce_sum | solution.py:78
  (32 shorter events, 0.2 us)
Async XLA Ops:
  7.2 118.3 %copy-start = (bf16[256,2048]{1,0:T(8,128)(2,1)S(1)}, bf16[256,2048]{1,0:T(8,128)(2,1)}, u32[]{:S(2)}) copy-start(bf16[256,2048]{1,0:T(8,128)(2,1)} %param.16) | copy-start | bytes 3145732
  7.2 21.9 %all-gather.2.cloned.1.call-start = ((), (), s32[]{:S(2)}) async-start(), calls=%async_computation.5 | async-start | bytes 1310720 | tf_op jit(solution)/shard_map/all_gather | solution.py:40
  7.9 148.7 %reduce-scatter.5.cloned.1.call-start = ((), (), s32[]{:S(2)}) async-start(), calls=%async_computation.6 | async-start | bytes 3932160 | tf_op jit(solution)/shard_map/reduce_scatter | solution.py:74
  63.5 11.4 %collective-permute-start.1 = (bf16[8,1,24,2048]{3,2,1,0:T(8,128)(2,1)S(1)}, bf16[8,1,24,2048]{3,2,1,0:T(8,128)(2,1)S(1)}, u32[]{:S(2)}, u32[]{:S(2)}) collective-permute-start(bf16[8,1,24,2048]{3,2,1,0:T(8,128)(2,1)S(1)} %all_to_all.10), channel_id=1, source_target_pairs={{0,1},{1,2},{2,3},{3,0},{4,5},{5,6},{6,7},{7,4},{8,9},{9,10},{10,1... | collective-permute-start | bytes 2359304 | tf_op jit(solution)/shard_map/ppermute | solution.py:66
  74.9 11.4 %collective-permute-start.2 = (bf16[8,1,24,2048]{3,2,1,0:T(8,128)(2,1)S(1)}, bf16[8,1,24,2048]{3,2,1,0:T(8,128)(2,1)S(1)}, u32[]{:S(2)}, u32[]{:S(2)}) collective-permute-start(bf16[8,1,24,2048]{3,2,1,0:T(8,128)(2,1)S(1)} %collective-permute-done.1), channel_id=1, source_target_pairs={{0,1},{1,2},{2,3},{3,0},{4,5},{5,6},{6,7},{7,4},{8,9},{9,10},{10,1... | collective-permute-start | bytes 2359304 | tf_op jit(solution)/shard_map/ppermute | solution.py:66
  86.3 11.5 %collective-permute-start.3 = (bf16[8,1,24,2048]{3,2,1,0:T(8,128)(2,1)S(1)}, bf16[8,1,24,2048]{3,2,1,0:T(8,128)(2,1)}, u32[]{:S(2)}, u32[]{:S(2)}) collective-permute-start(bf16[8,1,24,2048]{3,2,1,0:T(8,128)(2,1)S(1)} %collective-permute-done.2), channel_id=1, source_target_pairs={{0,1},{1,2},{2,3},{3,0},{4,5},{5,6},{6,7},{7,4},{8,9},{9,10},{10,1... | collective-permute-start | bytes 2359304 | tf_op jit(solution)/shard_map/ppermute | solution.py:66
  99.2 4.3 %copy-start.7 = (bf16[1,2048,896]{2,1,0:T(8,128)(2,1)S(1)}, bf16[1,2048,896]{2,1,0:T(8,128)(2,1)}, u32[]{:S(2)}) copy-start(bf16[1,2048,896]{2,1,0:T(8,128)(2,1)} %param.21) | copy-start | bytes 11010052
  100.8 2.7 %copy-start.4 = (bf16[8,1,192,2048]{3,2,1,0:T(8,128)(2,1)}, bf16[8,1,192,2048]{3,2,1,0:T(8,128)(2,1)S(1)}, u32[]{:S(2)}) copy-start(bf16[8,1,192,2048]{3,2,1,0:T(8,128)(2,1)S(1)} %constant_dynamic-update-slice_fusion) | copy-start | bytes 18874372
  108.4 12.3 %copy-start.1 = (bf16[256,256]{1,0:T(8,128)(2,1)S(1)}, bf16[256,256]{1,0:T(8,128)(2,1)}, u32[]{:S(2)}) copy-start(bf16[256,256]{1,0:T(8,128)(2,1)} %param.13) | copy-start | bytes 393220
  108.4 12.3 %copy-start.2 = (bf16[256,256]{1,0:T(8,128)(2,1)S(1)}, bf16[256,256]{1,0:T(8,128)(2,1)}, u32[]{:S(2)}) copy-start(bf16[256,256]{1,0:T(8,128)(2,1)} %param.14) | copy-start | bytes 393220
  108.4 15.7 %copy-start.5 = (f32[3,256]{1,0:T(4,128)S(1)}, f32[3,256]{1,0:T(4,128)}, u32[]{:S(2)}) copy-start(f32[3,256]{1,0:T(4,128)} %param.15) | copy-start | bytes 9220
  120.6 4.9 %copy-start.3 = (bf16[256,256]{1,0:T(8,128)(2,1)S(1)}, bf16[256,256]{1,0:T(8,128)(2,1)}, u32[]{:S(2)}) copy-start(bf16[256,256]{1,0:T(8,128)(2,1)} %param.12) | copy-start | bytes 393220
  120.6 41.5 %copy-start.6 = (f32[256,2]{0,1:T(2,128)S(1)}, f32[256,2]{0,1:T(2,128)}, u32[]{:S(2)}) copy-start(f32[256,2]{0,1:T(2,128)} %param.20) | copy-start | bytes 6148
  120.7 66.2 %reduce-scatter.3.cloned.1.call-start = ((), (), s32[]{:S(2)}) async-start(), calls=%async_computation.4 | async-start | bytes 1310720 | tf_op jit(solution)/shard_map/reduce_scatter | solution.py:31
  120.8 4.7 %collective-permute-start = (bf16[2,2,256]{2,1,0:T(2,128)(2,1)S(1)}, bf16[2,2,256]{2,1,0:T(2,128)(2,1)S(1)}, u32[]{:S(2)}, u32[]{:S(2)}) collective-permute-start(bf16[2,2,256]{2,1,0:T(2,128)(2,1)S(1)} %pad_maximum_fusion), channel_id=1, source_target_pairs={{0,4},{4,8},{8,12},{12,16},{16,20},{20,24},{24,28},{1,5},{5,9},{9,... | collective-permute-start | bytes 6152 | tf_op jit(solution)/shard_map/ppermute | solution.py:10
  156.7 25.6 %all-to-all-start.1 = ((bf16[8,1,96,512]{3,2,1,0:T(8,128)(2,1)}), bf16[8,1,96,512]{3,2,1,0:T(8,128)(2,1)S(1)}, u32[]{:S(2)}, u32[]{:S(2)}) async-start(bf16[8,1,96,512]{3,2,1,0:T(8,128)(2,1)} %bitcast.105), calls=%async_computation.3 | async-start | bytes 1572864 | tf_op jit(solution)/shard_map/all_to_all | solution.py:75
Sparse Core Ops, SparseCore 0:
  9.5 19.4 all-gather.1
  120.8 35.8 reduce-scatter.4
  159.8 24.8 reduce-scatter.2
